TPU v7x, 32 devices: a whole 2x2x4 slice. The times are simulated.
32 devices in a mesh: fs: 16 (over z, y, core), tp: 2 (over x).
Axes of the slice: x: 2, y: 2, z: 4, core: 2. Of those that a mesh axis runs over, the one named last changes fastest.
Arguments:
- inputs: bfloat16 [16384, 3072], P('fs'), may hold values from -6 to 6
- query_cot: bfloat16 [16384, 768], P('fs', 'tp'), may hold values from -0.046875 to 0.046875
- value_cot: bfloat16 [16384, 1536], P('fs', 'tp'), may hold values from -0.046875 to 0.046875
- query_factor: bfloat16 [3072, 192], P('fs'), may hold values from -0.109375 to 0.109375
- value_factor: bfloat16 [3072, 192], P('fs'), may hold values from -0.109375 to 0.109375
- query_weight: float32 [3072, 768], P('fs', 'tp'), may hold values from -0.109375 to 0.109375
- value_weight: float32 [3072, 1536], P('fs', 'tp'), may hold values from -0.109375 to 0.109375
- query_first: float32 [192, 768], P('fs', 'tp'), may hold values from -1.6 to 1.6
- query_second: float32 [192, 768], P('fs', 'tp'), may hold values from 0.002 to 0.05
- value_first: float32 [192, 1536], P('fs', 'tp'), may hold values from -1.6 to 1.6
- value_second: float32 [192, 1536], P('fs', 'tp'), may hold values from 0.002 to 0.05
Outputs:
- step_q: float32 [3072, 768], P('fs', 'tp')
- step_v: float32 [3072, 1536], P('fs', 'tp')
- new_q: float32 [3072, 768], P('fs', 'tp')
- new_v: float32 [3072, 1536], P('fs', 'tp')
- first_q: float32 [192, 768], P('fs', 'tp')
- second_q: float32 [192, 768], P('fs', 'tp')
- first_v: float32 [192, 1536], P('fs', 'tp')
- second_v: float32 [192, 1536], P('fs', 'tp')
- copy_q: bfloat16 [3072, 768], P(None, 'tp')
- copy_v: bfloat16 [3072, 1536], P(None, 'tp')
All inputs are finite; a program needn't handle non-finite values.
Results may differ from a plain program's by a relative error of at most 0.0041.
Values may be sent and summed in bfloat16 or wider, within the bound.
A program may use at most 64 MiB of HBM per device.

v0:
```python
import jax
import jax.numpy as jnp
from jax import lax
from jax.sharding import PartitionSpec as P

first_decay = 0.9
second_decay = 0.99
small_eps = 1e-08
learn_rate = 0.01


def moments(old_first, old_second, gradient):
    first = first_decay * old_first + (1.0 - first_decay) * gradient
    second = second_decay * old_second + (1.0 - second_decay) * gradient * gradient
    unit = first / (jnp.sqrt(second) + small_eps)
    return (first, second, unit)


def on_device(
    inputs,
    query_cot,
    value_cot,
    query_factor,
    value_factor,
    query_weight,
    value_weight,
    query_first,
    query_second,
    value_first,
    value_second,
):
    rank_cols = query_factor.shape[1]
    q_cols = query_cot.shape[1]
    v_cols = value_cot.shape[1]
    own_rows = query_first.shape[0]
    entries = rank_cols * (q_cols + v_cols) * lax.axis_size("tp")
    full_qf, full_vf = (
        lax.all_gather(query_factor, "fs", axis=0, tiled=True),
        lax.all_gather(value_factor, "fs", axis=0, tiled=True),
    )
    sum_q = jnp.dot(inputs, full_qf, preferred_element_type=jnp.float32)
    sum_v = jnp.dot(inputs, full_vf, preferred_element_type=jnp.float32)
    proj_q = sum_q.astype(jnp.bfloat16)
    proj_v = sum_v.astype(jnp.bfloat16)
    term_q = lax.dot_general(
        proj_q, query_cot, (((0,), (0,)), ((), ())), preferred_element_type=jnp.float32
    )
    term_v = lax.dot_general(
        proj_v, value_cot, (((0,), (0,)), ((), ())), preferred_element_type=jnp.float32
    )
    full_sums = lax.psum(jnp.concatenate([term_q, term_v], axis=1), "fs")
    stacked = (
        lax.all_gather(query_first, "fs", axis=0, tiled=True),
        lax.all_gather(query_second, "fs", axis=0, tiled=True),
        lax.all_gather(value_first, "fs", axis=0, tiled=True),
        lax.all_gather(value_second, "fs", axis=0, tiled=True),
    )
    all_first_q, all_second_q, unit_q = moments(stacked[0], stacked[1], full_sums[:, :q_cols])
    all_first_v, all_second_v, unit_v = moments(stacked[2], stacked[3], full_sums[:, q_cols:])
    norm_total = lax.psum(jnp.sum(unit_q * unit_q) + jnp.sum(unit_v * unit_v), "tp")
    step_scale = lax.rsqrt(norm_total / entries + 1e-06)
    whole_q = (step_scale * unit_q).astype(jnp.bfloat16)
    whole_v = (step_scale * unit_v).astype(jnp.bfloat16)
    row_begin = lax.axis_index("fs") * own_rows
    first_q = lax.dynamic_slice_in_dim(all_first_q, row_begin, own_rows, 0)
    second_q = lax.dynamic_slice_in_dim(all_second_q, row_begin, own_rows, 0)
    first_v = lax.dynamic_slice_in_dim(all_first_v, row_begin, own_rows, 0)
    second_v = lax.dynamic_slice_in_dim(all_second_v, row_begin, own_rows, 0)
    step_q = jnp.dot(query_factor, whole_q, preferred_element_type=jnp.float32)
    step_v = jnp.dot(value_factor, whole_v, preferred_element_type=jnp.float32)
    new_q = query_weight - learn_rate * step_q
    new_v = value_weight - learn_rate * step_v
    copy_q, copy_v = (
        lax.all_gather(new_q.astype(jnp.bfloat16), "fs", axis=0, tiled=True),
        lax.all_gather(new_v.astype(jnp.bfloat16), "fs", axis=0, tiled=True),
    )
    return (step_q, step_v, new_q, new_v, first_q, second_q, first_v, second_v, copy_q, copy_v)


def solution(mesh):
    in_specs = (
        P("fs", None),
        P("fs", "tp"),
        P("fs", "tp"),
        P("fs", None),
        P("fs", None),
        P("fs", "tp"),
        P("fs", "tp"),
        P("fs", "tp"),
        P("fs", "tp"),
        P("fs", "tp"),
        P("fs", "tp"),
    )
    out_specs = (
        P("fs", "tp"),
        P("fs", "tp"),
        P("fs", "tp"),
        P("fs", "tp"),
        P("fs", "tp"),
        P("fs", "tp"),
        P("fs", "tp"),
        P("fs", "tp"),
        P(None, "tp"),
        P(None, "tp"),
    )
    return jax.shard_map(
        on_device, mesh=mesh, in_specs=in_specs, out_specs=out_specs, check_vma=False
    )
```

profile of v0, /device:TPU:0, one launch (start us, length us, event | category | flops | bytes accessed | tf_op | source)
XLA Modules:
  0.0 321.6 jit_solution(11538157095303594677)
XLA Ops:
  8.0 0.7 all-gather.9.cloned.1.call-update
  8.7 24.6 %all-gather = f32[16,12,384]{2,1,0:T(8,128)S(1)} all-gather(f32[1,12,384]{2,1,0:T(8,128)} %bitcast.18), channel_id=1, replica_groups=mesh['fs'=16,'tp'=2] {'fs'}, dimensions={0}, use_global_device_ids=true | all-gather | bytes 313344 | tf_op jit(solution)/shard_map/all_gather | solution.py:53
  33.4 21.9 %all-gather.2 = f32[16,12,768]{2,1,0:T(8,128)S(1)} all-gather(f32[1,12,768]{2,1,0:T(8,128)} %bitcast.16), channel_id=1, replica_groups=mesh['fs'=16,'tp'=2] {'fs'}, dimensions={0}, use_global_device_ids=true | all-gather | bytes 626688 | tf_op jit(solution)/shard_map/all_gather | solution.py:55
  55.4 21.1 %all-gather.3 = f32[16,12,768]{2,1,0:T(8,128)S(1)} all-gather(f32[1,12,768]{2,1,0:T(8,128)S(1)} %bitcast.17), channel_id=1, replica_groups=mesh['fs'=16,'tp'=2] {'fs'}, dimensions={0}, use_global_device_ids=true | all-gather | bytes 626688 | tf_op jit(solution)/shard_map/all_gather | solution.py:56
  76.6 6.6 %fusion.1 = f32[192,768]{1,0:T(8,128)} fusion(bf16[1024,768]{1,0:T(8,128)(2,1)S(1)} %copy-done, bf16[1024,3072]{1,0:T(8,128)(2,1)} %param.11, bf16[3072,192]{1,0:T(8,128)(2,1)} %all-gather.11.cloned.1.call-done), kind=kOutput, calls=%fused_computation.5 | convolution fusion | flops 1510146048 | bytes 9633792 | tf_op jit(solution)/shard_map/dot_general | solution.py:48
  83.3 15.3 %all-gather.9.cloned.1.call-done = bf16[3072,192]{1,0:T(8,128)(2,1)} async-done(((bf16[192,192]{1,0:T(8,128)(2,1)}), bf16[3072,192]{1,0:T(8,128)(2,1)}) %all-gather.9.cloned.1.call-update) | async-done | bytes 1179664 | tf_op jit(solution)/shard_map/all_gather | solution.py:38
  98.5 6.5 %fusion = f32[192,384]{1,0:T(8,128)} fusion(bf16[1024,384]{1,0:T(8,128)(2,1)} %param.12, bf16[1024,3072]{1,0:T(8,128)(2,1)} %param.11, bf16[3072,192]{1,0:T(8,128)(2,1)} %all-gather.9.cloned.1.call-done), kind=kOutput, calls=%fused_computation.4 | convolution fusion | flops 1359151104 | bytes 8552448 | tf_op jit(solution)/shard_map/dot_general | solution.py:45
  105.0 2.1 pad_maximum_fusion
  107.2 0.8 broadcast_multiply_fusion.3
  108.0 0.9 reshape.33
  108.9 0.9 reshape.35
  110.0 0.7 reshape.29
  110.7 20.7 %all-gather.1 = f32[16,12,384]{2,1,0:T(8,128)S(1)} all-gather(f32[1,12,384]{2,1,0:T(8,128)S(1)} %bitcast.19), channel_id=1, replica_groups=mesh['fs'=16,'tp'=2] {'fs'}, dimensions={0}, use_global_device_ids=true | all-gather | bytes 313344 | tf_op jit(solution)/shard_map/all_gather | solution.py:54
  131.4 0.7 reshape.31
  132.2 67.6 %all-reduce.2.cloned.1.call-done = f32[192,1152]{1,0:T(8,128)} async-done(((f32[192,1152]{1,0:T(8,128)}), f32[192,1152]{1,0:T(8,128)}) %all-reduce.2.cloned.1.call-update) | async-done | bytes 884752 | tf_op jit(solution)/shard_map/psum | solution.py:51
  199.7 2.2 multiply_reduce_fusion
  202.0 1.8 multiply_reduce_fusion.1
  205.1 5.4 %psum.15 = f32[]{:T(128)} all-reduce(f32[]{:T(128)S(6)} %add.48), channel_id=1, replica_groups=mesh['fs'=16,'tp'=2] {'tp'}, use_global_device_ids=true, to_apply=%region_3.0 | all-reduce | flops 1 | bytes 8 | tf_op jit(solution)/shard_map/psum | solution.py:60
  211.2 2.1 fusion.7
  213.4 2.6 fusion.6
  217.3 37.5 %all-gather.13.cloned.1.call-done = bf16[3072,384]{1,0:T(8,128)(2,1)} async-done(((bf16[192,384]{1,0:T(8,128)(2,1)}), bf16[3072,384]{1,0:T(8,128)(2,1)}) %all-gather.13.cloned.1.call-update) | async-done | bytes 2359312 | tf_op jit(solution)/shard_map/all_gather | solution.py:74
  254.8 54.6 %all-gather.15.cloned.1.call-done = bf16[3072,768]{1,0:T(8,128)(2,1)} async-done(((bf16[192,768]{1,0:T(8,128)(2,1)}), bf16[3072,768]{1,0:T(8,128)(2,1)}) %all-gather.15.cloned.1.call-update) | async-done | bytes 4718608 | tf_op jit(solution)/shard_map/all_gather | solution.py:75
  309.4 3.5 %copy.24 = bf16[3072,384]{1,0:T(8,128)(2,1)} copy(bf16[3072,384]{1,0:T(8,128)(2,1)} %all-gather.13.cloned.1.call-done) | data formatting | bytes 4718592
  312.8 2.2 copy.25
  (35 shorter events, 2.6 us)
Async XLA Ops:
  7.2 69.5 %copy-start = (bf16[1024,768]{1,0:T(8,128)(2,1)S(1)}, bf16[1024,768]{1,0:T(8,128)(2,1)}, u32[]{:S(2)}) copy-start(bf16[1024,768]{1,0:T(8,128)(2,1)} %param.13) | copy-start | bytes 4718596
  7.2 48.2 %copy-start.8 = (f32[12,768]{1,0:T(8,128)S(1)}, f32[12,768]{1,0:T(8,128)}, u32[]{:S(2)}) copy-start(f32[12,768]{1,0:T(8,128)} %param.21) | copy-start | bytes 110596
  7.2 69.4 %all-gather.11.cloned.1.call-start = ((), (), s32[]{:S(2)}) async-start(), calls=%async_computation.1 | async-start | bytes 1671168 | tf_op jit(solution)/shard_map/all_gather | solution.py:39
  7.9 90.6 %all-gather.9.cloned.1.call-start = ((), (), s32[]{:S(2)}) async-start(), calls=%async_computation | async-start | bytes 1671168 | tf_op jit(solution)/shard_map/all_gather | solution.py:38
  8.7 191.0 %all-reduce.2.cloned.1.call-start = ((), (), s32[]{:S(2)}) async-start(), calls=%async_computation.2 | async-start | bytes 1769472 | tf_op jit(solution)/shard_map/psum | solution.py:51
  107.2 147.6 %all-gather.13.cloned.1.call-start = ((), (), s32[]{:S(2)}) async-start(), calls=%async_computation.3 | async-start | bytes 2506752 | tf_op jit(solution)/shard_map/all_gather | solution.py:74
  108.9 1.1 copy-start.3
  108.9 1.8 copy-start.9
  110.0 89.8 %copy-start.2 = (f32[192,768]{1,0:T(8,128)S(1)}, f32[192,768]{1,0:T(8,128)}, u32[]{:S(2)}) copy-start(f32[192,768]{1,0:T(8,128)} %reshape.33) | copy-start | bytes 1769476
  132.2 79.0 %copy-start.7 = (bf16[192,192]{1,0:T(8,128)(2,1)S(1)}, bf16[192,192]{1,0:T(8,128)(2,1)}, u32[]{:S(2)}) copy-start(bf16[192,192]{1,0:T(8,128)(2,1)} %param.14) | copy-start | bytes 221188
  199.7 2.2 copy-start.4
  199.7 2.2 copy-start.5
  202.0 11.4 %copy-start.6 = (bf16[192,192]{1,0:T(8,128)(2,1)S(1)}, bf16[192,192]{1,0:T(8,128)(2,1)}, u32[]{:S(2)}) copy-start(bf16[192,192]{1,0:T(8,128)(2,1)} %param.15) | copy-start | bytes 221188
  213.3 96.0 %all-gather.15.cloned.1.call-start = ((), (), s32[]{:S(2)}) async-start(), calls=%async_computation.4 | async-start | bytes 5013504 | tf_op jit(solution)/shard_map/all_gather | solution.py:75
  309.4 3.5 %copy-start.1 = (bf16[3072,768]{1,0:T(8,128)(2,1)S(1)}, bf16[3072,768]{1,0:T(8,128)(2,1)}, u32[]{:S(2)}) copy-start(bf16[3072,768]{1,0:T(8,128)(2,1)} %all-gather.15.cloned.1.call-done) | copy-start | bytes 14155780
Sparse Core Ops, SparseCore 0:
  10.3 43.8 all-gather.10
  56.4 42.0 all-gather.8
  107.3 92.3 all-reduce.1
  213.5 41.3 all-gather.12
  257.5 51.8 all-gather.14
where the time goes:
time: 322 us
  waiting for transfers between devices  176 us (55%)
  blocking collectives  93.8 us (29%)
  matrix products  17.9 us (6%)
  between operations  15.9 us (5%)
  local copies, waits for them, and re-layouts  10.4 us (3%)
  other arithmetic  7.08 us (2%)
    psum x1, waiting for transfers between devices, on_device(): full_sums = lax.psum(jnp.concatenate([term_q, term_v], axis=1), 'fs')  67.6 us
    all_gather x1, waiting for transfers between devices, on_device(): lax.all_gather(new_v.astype(jnp.bfloat16), 'fs', axis=0, tiled=True)  54.6 us
    all_gather x1, waiting for transfers between devices, on_device(): lax.all_gather(new_q.astype(jnp.bfloat16), 'fs', axis=0, tiled=True)  37.5 us
    all_gather x1, blocking collectives, on_device(): lax.all_gather(query_first, 'fs', axis=0, tiled=True)  24.6 us
    all_gather x1, blocking collectives, on_device(): lax.all_gather(value_first, 'fs', axis=0, tiled=True)  21.9 us
    all_gather x1, blocking collectives, on_device(): lax.all_gather(value_second, 'fs', axis=0, tiled=True)  21.1 us
    all_gather x1, blocking collectives, on_device(): lax.all_gather(query_second, 'fs', axis=0, tiled=True)  20.7 us
    all_gather x1, waiting for transfers between devices, on_device(): lax.all_gather(query_factor, 'fs', axis=0, tiled=True)  15.3 us
  transfers between devices with their start and end apart: 5, of which 4 were waited for; matrix products, arithmetic and copies ran while one was open for 5% of the time, Pallas kernels for 0%

commit v1 on v0

--- a/solution.py
+++ b/solution.py
@@ -72,7 +72,12 @@
     new_v = value_weight - learn_rate * step_v
     copy_q, copy_v = (
         lax.all_gather(new_q.astype(jnp.bfloat16), "fs", axis=0, tiled=True),
-        lax.all_gather(new_v.astype(jnp.bfloat16), "fs", axis=0, tiled=True),
+        jnp.concatenate(
+            lax.all_to_all(
+                jnp.stack([new_v.astype(jnp.bfloat16)] * lax.axis_size("fs")), "fs", 0, 0
+            ),
+            axis=0,
+        ),
     )
     return (step_q, step_v, new_q, new_v, first_q, second_q, first_v, second_v, copy_q, copy_v)
 

time: 322 us -> 353 us (1.096)
  the two profiles are of different devices: /device:TPU:0 before, /device:TPU:13 now
where the time goes in v1:
time: 353 us
  waiting for transfers between devices  201 us (57%)
  blocking collectives  86.6 us (25%)
  matrix products  17.8 us (5%)
  between operations  15.9 us (5%)
  local copies, waits for them, and re-layouts  15.3 us (4%)
  starting transfers between devices  8.9 us (3%)
  other arithmetic  7.12 us (2%)
    all_gather x1, waiting for transfers between devices, on_device(): lax.all_gather(new_q.astype(jnp.bfloat16), 'fs', axis=0, tiled=True)  91.2 us
    psum x1, waiting for transfers between devices, on_device(): full_sums = lax.psum(jnp.concatenate([term_q, term_v], axis=1), 'fs')  69.2 us
    all_gather x1, blocking collectives, on_device(): lax.all_gather(value_first, 'fs', axis=0, tiled=True)  26.4 us
    all_to_all x1, waiting for transfers between devices, on_device(): lax.all_to_all(jnp.stack([new_v.astype(jnp.bfloat16)] * lax.axis_size('fs...  23.2 us
    all_gather x1, blocking collectives, on_device(): lax.all_gather(value_second, 'fs', axis=0, tiled=True)  20.6 us
    all_gather x1, blocking collectives, on_device(): lax.all_gather(query_second, 'fs', axis=0, tiled=True)  18.4 us
    all_gather x1, blocking collectives, on_device(): lax.all_gather(query_first, 'fs', axis=0, tiled=True)  16.9 us
    all_gather x1, waiting for transfers between devices, on_device(): lax.all_gather(query_factor, 'fs', axis=0, tiled=True)  15.9 us
  transfers between devices with their start and end apart: 5, of which 4 were waited for; matrix products, arithmetic and copies ran while one was open for 4% of the time, Pallas kernels for 0%

profile of v1, /device:TPU:13, one launch (start us, length us, event | category | flops | bytes accessed | tf_op | source)
XLA Modules:
  0.0 352.6 jit_solution(1083909091659549428)
XLA Ops:
  8.7 16.9 %all-gather = f32[16,12,384]{2,1,0:T(8,128)S(1)} all-gather(f32[1,12,384]{2,1,0:T(8,128)} %bitcast.19), channel_id=1, replica_groups=mesh['fs'=16,'tp'=2] {'fs'}, dimensions={0}, use_global_device_ids=true | all-gather | bytes 313344 | tf_op jit(solution)/shard_map/all_gather | solution.py:53
  25.7 26.4 %all-gather.2 = f32[16,12,768]{2,1,0:T(8,128)S(1)} all-gather(f32[1,12,768]{2,1,0:T(8,128)} %bitcast.17), channel_id=1, replica_groups=mesh['fs'=16,'tp'=2] {'fs'}, dimensions={0}, use_global_device_ids=true | all-gather | bytes 626688 | tf_op jit(solution)/shard_map/all_gather | solution.py:55
  52.2 20.6 %all-gather.3 = f32[16,12,768]{2,1,0:T(8,128)S(1)} all-gather(f32[1,12,768]{2,1,0:T(8,128)S(1)} %bitcast.18), channel_id=1, replica_groups=mesh['fs'=16,'tp'=2] {'fs'}, dimensions={0}, use_global_device_ids=true | all-gather | bytes 626688 | tf_op jit(solution)/shard_map/all_gather | solution.py:56
  72.9 6.6 %fusion.1 = f32[192,768]{1,0:T(8,128)} fusion(bf16[1024,768]{1,0:T(8,128)(2,1)S(1)} %copy-done, bf16[1024,3072]{1,0:T(8,128)(2,1)} %param.11, bf16[3072,192]{1,0:T(8,128)(2,1)} %all-gather.10.cloned.1.call-done), kind=kOutput, calls=%fused_computation.5 | convolution fusion | flops 1510146048 | bytes 9633792 | tf_op jit(solution)/shard_map/dot_general | solution.py:48
  79.5 15.9 %all-gather.8.cloned.1.call-done = bf16[3072,192]{1,0:T(8,128)(2,1)} async-done(((bf16[192,192]{1,0:T(8,128)(2,1)}), bf16[3072,192]{1,0:T(8,128)(2,1)}) %all-gather.8.cloned.1.call-update) | async-done | bytes 1179664 | tf_op jit(solution)/shard_map/all_gather | solution.py:38
  95.4 6.5 %fusion = f32[192,384]{1,0:T(8,128)} fusion(bf16[1024,384]{1,0:T(8,128)(2,1)} %param.12, bf16[1024,3072]{1,0:T(8,128)(2,1)} %param.11, bf16[3072,192]{1,0:T(8,128)(2,1)} %all-gather.8.cloned.1.call-done), kind=kOutput, calls=%fused_computation.4 | convolution fusion | flops 1359151104 | bytes 8552448 | tf_op jit(solution)/shard_map/dot_general | solution.py:45
  102.0 2.1 pad_maximum_fusion
  104.1 0.8 broadcast_multiply_fusion.3
  104.9 0.9 reshape.39
  105.8 0.9 reshape.41
  107.4 18.4 %all-gather.1 = f32[16,12,384]{2,1,0:T(8,128)S(1)} all-gather(f32[1,12,384]{2,1,0:T(8,128)} %bitcast.20), channel_id=1, replica_groups=mesh['fs'=16,'tp'=2] {'fs'}, dimensions={0}, use_global_device_ids=true | all-gather | bytes 313344 | tf_op jit(solution)/shard_map/all_gather | solution.py:54
  125.9 0.7 reshape.37
  126.6 69.2 %all-reduce.2.cloned.1.call-done = f32[192,1152]{1,0:T(8,128)} async-done(((f32[192,1152]{1,0:T(8,128)}), f32[192,1152]{1,0:T(8,128)}) %all-reduce.2.cloned.1.call-update) | async-done | bytes 884752 | tf_op jit(solution)/shard_map/psum | solution.py:51
  195.8 2.2 multiply_reduce_fusion
  198.0 1.8 multiply_reduce_fusion.1
  201.2 4.3 %psum.15 = f32[]{:T(128)} all-reduce(f32[]{:T(128)S(6)} %add.48), channel_id=1, replica_groups=mesh['fs'=16,'tp'=2] {'tp'}, use_global_device_ids=true, to_apply=%region_3.0 | all-reduce | flops 1 | bytes 8 | tf_op jit(solution)/shard_map/psum | solution.py:60
  206.1 2.5 fusion.6
  208.7 2.6 stack.2
  211.3 8.7 %all-to-all-start = ((bf16[16,192,768]{2,1,0:T(8,128)(2,1)}), bf16[16,192,768]{2,1,0:T(8,128)(2,1)}, u32[]{:S(2)}, u32[]{:S(2)}) async-start(bf16[16,192,768]{2,1,0:T(8,128)(2,1)} %stack.2), calls=%async_computation | async-start | bytes 9437184 | tf_op jit(solution)/shard_map/all_to_all | solution.py:76
  220.1 2.1 fusion.7
  223.5 91.2 %all-gather.12.cloned.1.call-done = bf16[3072,384]{1,0:T(8,128)(2,1)} async-done(((bf16[192,384]{1,0:T(8,128)(2,1)}), bf16[3072,384]{1,0:T(8,128)(2,1)}) %all-gather.12.cloned.1.call-update) | async-done | bytes 2359312 | tf_op jit(solution)/shard_map/all_gather | solution.py:74
  314.7 23.2 %all-to-all-done = bf16[16,192,768]{2,1,0:T(8,128)(2,1)} async-done(((bf16[16,192,768]{2,1,0:T(8,128)(2,1)}), bf16[16,192,768]{2,1,0:T(8,128)(2,1)}, u32[]{:S(2)}, u32[]{:S(2)}) %all-to-all-start) | async-done | bytes 4718624 | tf_op jit(solution)/shard_map/all_to_all | solution.py:76
  337.9 3.3 copy.24
  341.2 4.8 %copy.25 = bf16[3072,768]{1,0:T(8,128)(2,1)} copy(bf16[3072,768]{1,0:T(8,128)(2,1)} %bitcast.6) | data formatting | bytes 9437184
  (29 shorter events, 3.8 us)
Async XLA Ops:
  7.2 65.7 %copy-start = (bf16[1024,768]{1,0:T(8,128)(2,1)S(1)}, bf16[1024,768]{1,0:T(8,128)(2,1)}, u32[]{:S(2)}) copy-start(bf16[1024,768]{1,0:T(8,128)(2,1)} %param.13) | copy-start | bytes 4718596
  7.2 45.0 %copy-start.6 = (f32[12,768]{1,0:T(8,128)S(1)}, f32[12,768]{1,0:T(8,128)}, u32[]{:S(2)}) copy-start(f32[12,768]{1,0:T(8,128)} %param.21) | copy-start | bytes 110596
  7.2 65.7 %all-gather.10.cloned.1.call-start = ((), (), s32[]{:S(2)}) async-start(), calls=%async_computation.2 | async-start | bytes 1671168 | tf_op jit(solution)/shard_map/all_gather | solution.py:39
  7.9 87.5 %all-gather.8.cloned.1.call-start = ((), (), s32[]{:S(2)}) async-start(), calls=%async_computation.1 | async-start | bytes 1671168 | tf_op jit(solution)/shard_map/all_gather | solution.py:38
  8.7 187.1 %all-reduce.2.cloned.1.call-start = ((), (), s32[]{:S(2)}) async-start(), calls=%async_computation.3 | async-start | bytes 1769472 | tf_op jit(solution)/shard_map/psum | solution.py:51
  104.9 1.8 copy-start.2
  106.6 89.2 %copy-start.1 = (f32[192,768]{1,0:T(8,128)S(1)}, f32[192,768]{1,0:T(8,128)}, u32[]{:S(2)}) copy-start(f32[192,768]{1,0:T(8,128)} %reshape.39) | copy-start | bytes 1769476
  126.6 79.5 %copy-start.4 = (bf16[192,192]{1,0:T(8,128)(2,1)S(1)}, bf16[192,192]{1,0:T(8,128)(2,1)}, u32[]{:S(2)}) copy-start(bf16[192,192]{1,0:T(8,128)(2,1)} %param.15) | copy-start | bytes 221188
  195.8 2.2 copy-start.3
  211.3 8.8 %copy-start.5 = (bf16[192,192]{1,0:T(8,128)(2,1)S(1)}, bf16[192,192]{1,0:T(8,128)(2,1)}, u32[]{:S(2)}) copy-start(bf16[192,192]{1,0:T(8,128)(2,1)} %param.14) | copy-start | bytes 221188
  211.3 126.6 %all-to-all-start = ((bf16[16,192,768]{2,1,0:T(8,128)(2,1)}), bf16[16,192,768]{2,1,0:T(8,128)(2,1)}, u32[]{:S(2)}, u32[]{:S(2)}) async-start(bf16[16,192,768]{2,1,0:T(8,128)(2,1)} %stack.2), calls=%async_computation | async-start | bytes 9437184 | tf_op jit(solution)/shard_map/all_to_all | solution.py:76
  220.0 94.7 %all-gather.12.cloned.1.call-start = ((), (), s32[]{:S(2)}) async-start(), calls=%async_computation.4 | async-start | bytes 2506752 | tf_op jit(solution)/shard_map/all_gather | solution.py:74
Sparse Core Ops, SparseCore 0:
  10.3 43.6 all-gather.9
  56.2 39.1 all-gather.7
  104.2 91.5 all-reduce.1
  223.4 91.2 all-gather.11
